TPU v7x, 128 devices: a whole 4x4x4 slice. The times are simulated.
128 devices in a mesh: ra: 16 (over z, x), cb: 4 (over y), dp: 2 (over core).
Axes of the slice: x: 4, y: 4, z: 4, core: 2. Of those that a mesh axis runs over, the one named last changes fastest.
Arguments:
- carried: bfloat16 [3072, 4096], P('dp', 'ra'), may hold values from -100 to 100
- branch_in: bfloat16 [3072, 4096], P('dp', 'ra'), may hold values from -12 to 12
- gain_in: float32 [4096], P('ra'), may hold values from 0.1 to 1.9
- bias_in: float32 [4096], P('ra'), may hold values from -1.8 to 1.8
- up_weight: bfloat16 [4096, 16384], P('ra', 'cb'), may hold values from -0.125 to 0.125
- down_weight: bfloat16 [16384, 4096], P('cb', 'ra'), may hold values from -0.046875 to 0.046875
- gain_out: float32 [4096], P('ra'), may hold values from 0.1 to 1.9
- bias_out: float32 [4096], P('ra'), may hold values from -1.8 to 1.8
Outputs:
- layer_out: bfloat16 [3072, 4096], P('dp', 'ra')
All inputs are finite; a program needn't handle non-finite values.
Results may differ from a plain program's by a relative error of at most 0.006.
Values may be sent and summed in bfloat16 or wider, within the bound.
A program may use at most 64 MiB of HBM per device.

v0:
```python
import jax
import jax.numpy as jnp
from jax import lax
from jax.sharding import PartitionSpec as P

residual_scale = 2.0**0.25
norm_eps = 1e-05


def copy_for_each(array, axis):
    length = lax.axis_size(axis)
    return lax.all_to_all(
        jnp.broadcast_to(array[None], (length, *array.shape)), axis, 0, 0, tiled=True
    )


def of_everyone(array, axis):
    return copy_for_each(array, axis).sum(axis=0)


def packed_total(arrays, axis):
    ravelled, at, done = (jnp.concatenate([a.reshape(-1) for a in arrays]), 0, [])
    running = of_everyone(ravelled, axis)
    for a in arrays:
        done.append(running[at : at + a.size].reshape(a.shape))
        at += a.size
    return tuple(done)


def taken_together(array, axis):
    return copy_for_each(array, axis).astype(jnp.float32).sum(axis=0)


def normalize(mixed, totals, squares, width, gain, bias):
    mean = totals[:, None] / width
    spread = squares[:, None] / width - mean * mean
    return (mixed - mean) * lax.rsqrt(spread + norm_eps) * gain + bias


def per_device(carried, branch_in, gain_in, bias_in, up_weight, down_weight, gain_out, bias_out):
    width = carried.shape[1] * lax.axis_size("ra")
    mixed_in = residual_scale * carried.astype(jnp.float32) + branch_in.astype(jnp.float32)
    totals, squares = packed_total(
        (jnp.sum(mixed_in, axis=1), jnp.sum(mixed_in * mixed_in, axis=1)), "ra"
    )
    normed = normalize(mixed_in, totals, squares, width, gain_in, bias_in).astype(jnp.bfloat16)
    regrouped = lax.all_to_all(up_weight, "ra", split_axis=1, concat_axis=0, tiled=True)
    pre_share = lax.dot_general(
        regrouped,
        lax.all_gather(normed, "ra", axis=1, tiled=True),
        (((0,), (1,)), ((), ())),
        preferred_element_type=jnp.float32,
    )
    hidden_share = jnp.square(jnp.maximum(pre_share, 0.0)).astype(jnp.bfloat16)
    branch_part = lax.dot_general(
        lax.all_gather(hidden_share, "ra", axis=0, tiled=True),
        down_weight,
        (((0,), (0,)), ((), ())),
        preferred_element_type=jnp.float32,
    )
    branch_out = taken_together(branch_part.astype(jnp.bfloat16), "cb").astype(jnp.float32)
    mixed_out = residual_scale * normed.astype(jnp.float32) + branch_out
    totals_out, squares_out = packed_total(
        (jnp.sum(mixed_out, axis=1), jnp.sum(mixed_out * mixed_out, axis=1)), "ra"
    )
    return normalize(mixed_out, totals_out, squares_out, width, gain_out, bias_out).astype(
        jnp.bfloat16
    )


def solution(mesh):
    in_specs = (
        P("dp", "ra"),
        P("dp", "ra"),
        P("ra"),
        P("ra"),
        P("ra", "cb"),
        P("cb", "ra"),
        P("ra"),
        P("ra"),
    )
    out_specs = P("dp", "ra")
    return jax.shard_map(
        per_device, mesh=mesh, in_specs=in_specs, out_specs=out_specs, check_vma=False
    )
```

profile of v0, /device:TPU:0, one launch (start us, length us, event | category | flops | bytes accessed | tf_op | source)
XLA Modules:
  0.0 324.9 jit_solution(11136814874928397678)
XLA Ops:
  6.5 0.0 copy-start
  6.5 0.0 copy-start.3
  6.5 0.0 copy-start.4
  6.5 0.0 copy-start.5
  6.5 0.0 all-gather.3.cloned.1.call-start
  6.6 2.1 fusion.3
  8.7 0.1 broadcast_in_dim.6
  8.8 16.1 %all_to_all.36 = f32[16,1,3072]{2,1,0:T(1,128)S(1)} all-to-all(f32[16,1,3072]{2,1,0:T(1,128)S(1)} %broadcast_in_dim.6), channel_id=1, replica_groups=mesh['ra'=16,'cb'=4,'dp'=2] {'ra'}, dimensions={0} | all-to-all | bytes 393216 | tf_op jit(solution)/shard_map/all_to_all | solution.py:12
  24.9 0.1 reduce_sum.65
  25.1 0.0 copy-done.3
  25.1 0.0 copy-done.4
  25.1 0.0 copy-done.5
  25.1 2.5 add_convert_fusion.1
  27.6 0.0 all-gather.3.cloned.1.call-update
  27.6 0.0 all-gather.5.cloned.1.call-start
  27.7 4.1 %copy.14 = bf16[256,4096]{0,1:T(8,128)(2,1)} copy(bf16[256,4096]{1,0:T(8,128)(2,1)} %param.12) | data formatting | bytes 4194304 | tf_op args[4]
  31.7 44.3 %all_to_all.37 = bf16[256,16,256]{0,2,1:T(8,128)(2,1)} all-to-all(bf16[256,16,256]{0,2,1:T(8,128)(2,1)} %bitcast.10), channel_id=1, replica_groups=mesh['ra'=16,'cb'=4,'dp'=2] {'ra'}, dimensions={1} | all-to-all | bytes 4194304 | tf_op jit(solution)/shard_map/all_to_all | solution.py:47
  76.0 3.9 %copy.15 = bf16[16,256,256]{2,1,0:T(8,128)(2,1)} copy(bf16[16,256,256]{1,2,0:T(8,128)(2,1)} %bitcast.9) | data formatting | bytes 4194304 | tf_op jit(solution)/shard_map/all_to_all | solution.py:47
  79.9 65.2 %all-gather.3.cloned.1.call-done = bf16[1536,4096]{1,0:T(8,128)(2,1)} async-done(((bf16[1536,256]{1,0:T(8,128)(2,1)}), bf16[1536,4096]{1,0:T(8,128)(2,1)}) %all-gather.3.cloned.1.call-update) | async-done | bytes 12582928 | tf_op jit(solution)/shard_map/all_gather | solution.py:50
  145.1 9.6 %fusion.2 = bf16[256,1536]{0,1:T(8,128)(2,1)} fusion(bf16[1536,4096]{1,0:T(8,128)(2,1)} %all-gather.3.cloned.1.call-done, bf16[4096,256]{1,0:T(8,128)(2,1)} %bitcast.11), kind=kOutput, calls=%fused_computation.5 | convolution fusion | flops 3222405120 | bytes 15466496 | tf_op jit(solution)/shard_map/dot_general | solution.py:48
  154.7 0.0 all-gather.5.cloned.1.call-update
  154.7 98.0 %all-gather.5.cloned.1.call-done = bf16[4096,1536]{0,1:T(8,128)(2,1)} async-done(((bf16[256,1536]{0,1:T(8,128)(2,1)}), bf16[4096,1536]{0,1:T(8,128)(2,1)}) %all-gather.5.cloned.1.call-update) | async-done | bytes 12582928 | tf_op jit(solution)/shard_map/all_gather | solution.py:56
  252.8 0.0 copy-done
  252.8 6.5 %convolution_convert_fusion = bf16[1536,256]{1,0:T(8,128)(2,1)S(1)} fusion(bf16[4096,1536]{0,1:T(8,128)(2,1)} %all-gather.5.cloned.1.call-done, bf16[4096,256]{1,0:T(8,128)(2,1)S(1)} %copy-done), kind=kOutput, calls=%fused_computation.4 | convolution fusion | flops 3221618688 | bytes 15466496 | tf_op jit(solution)/shard_map/dot_general | solution.py:55
  259.3 0.2 broadcast_in_dim.7
  259.5 40.3 %all_to_all.38 = bf16[4,1536,256]{2,1,0:T(8,128)(2,1)S(1)} all-to-all(bf16[4,1536,256]{2,1,0:T(8,128)(2,1)S(1)} %broadcast_in_dim.7), channel_id=1, replica_groups=mesh['ra'=16,'cb'=4,'dp'=2] {'cb'}, dimensions={0} | all-to-all | bytes 6291456 | tf_op jit(solution)/shard_map/all_to_all | solution.py:12
  299.8 0.0 copy-start.2
  299.8 0.5 convert_reduce_fusion
  300.2 0.0 copy-start.1
  300.2 1.1 copy-done.1
  301.4 0.0 copy-done.2
  301.4 0.0 copy-start.6
  301.4 0.0 copy-start.7
  301.4 0.5 fusion.4
  301.9 0.1 broadcast_in_dim.8
  302.0 13.1 %all_to_all.39 = f32[16,1,3072]{2,1,0:T(1,128)S(1)} all-to-all(f32[16,1,3072]{2,1,0:T(1,128)S(1)} %broadcast_in_dim.8), channel_id=1, replica_groups=mesh['ra'=16,'cb'=4,'dp'=2] {'ra'}, dimensions={0} | all-to-all | bytes 393216 | tf_op jit(solution)/shard_map/all_to_all | solution.py:12
  315.1 0.1 reduce_sum.69
  315.3 0.0 copy-done.6
  315.3 0.0 copy-done.7
  315.3 2.8 add_convert_fusion
  (4 shorter events, 0.0 us)
Async XLA Ops:
  6.5 246.2 %copy-start = (bf16[4096,256]{1,0:T(8,128)(2,1)S(1)}, bf16[4096,256]{1,0:T(8,128)(2,1)}, u32[]{:S(2)}) copy-start(bf16[4096,256]{1,0:T(8,128)(2,1)} %param.13) | copy-start | bytes 6291460
  6.5 18.5 %copy-start.3 = (bf16[1536,256]{1,0:T(8,128)(2,1)S(1)}, bf16[1536,256]{1,0:T(8,128)(2,1)}, u32[]{:S(2)}) copy-start(bf16[1536,256]{1,0:T(8,128)(2,1)} %param.9) | copy-start | bytes 2359300
  6.5 18.5 %copy-start.4 = (f32[256]{0:T(256)S(1)}, f32[256]{0:T(256)}, u32[]{:S(2)}) copy-start(f32[256]{0:T(256)} %param.11) | copy-start | bytes 3076
  6.5 18.5 %copy-start.5 = (f32[256]{0:T(256)S(1)}, f32[256]{0:T(256)}, u32[]{:S(2)}) copy-start(f32[256]{0:T(256)} %param.10) | copy-start | bytes 3076
  6.5 138.6 %all-gather.3.cloned.1.call-start = ((), (), s32[]{:S(2)}) async-start(), calls=%async_computation.4 | async-start | bytes 13369344 | tf_op jit(solution)/shard_map/all_gather | solution.py:50
  27.6 225.1 %all-gather.5.cloned.1.call-start = ((), (), s32[]{:S(2)}) async-start(), calls=%async_computation.5 | async-start | bytes 13369344 | tf_op jit(solution)/shard_map/all_gather | solution.py:56
  299.8 1.6 copy-start.2
  300.2 1.2 copy-start.1
  301.4 13.9 %copy-start.6 = (f32[256]{0:T(256)S(1)}, f32[256]{0:T(256)}, u32[]{:S(2)}) copy-start(f32[256]{0:T(256)} %param.15) | copy-start | bytes 3076
  301.4 13.9 %copy-start.7 = (f32[256]{0:T(256)S(1)}, f32[256]{0:T(256)}, u32[]{:S(2)}) copy-start(f32[256]{0:T(256)} %param.14) | copy-start | bytes 3076
Sparse Core Ops, SparseCore 0:
  27.7 117.3 all-gather.2
  154.9 97.8 all-gather.4
where the time goes:
time: 325 us
  waiting for transfers between devices  163 us (50%)
  blocking collectives  114 us (35%)
  matrix products  16.1 us (5%)
  between operations  13.5 us (4%)
  local copies, waits for them, and re-layouts  9.57 us (3%)
  other arithmetic  8.59 us (3%)
    all_gather x1, waiting for transfers between devices, per_device(): lax.all_gather(hidden_share, 'ra', axis=0, tiled=True)  98 us
    all_to_all x3, blocking collectives, copy_for_each(): lax.all_to_all(jnp.broadcast_to(array[None], (length, *array.shape)), axi...  69.5 us
    all_gather x1, waiting for transfers between devices, per_device(): lax.all_gather(normed, 'ra', axis=1, tiled=True)  65.2 us
    all_to_all x1, blocking collectives, per_device(): lax.all_to_all(up_weight, 'ra', split_axis=1, concat_axis=0, tiled=True)  44.3 us
    dot_general x1, matrix products, per_device(): lax.dot_general(regrouped, lax.all_gather(normed, 'ra', axis=1, tiled=Tru...  9.57 us
  transfers between devices with their start and end apart: 2, of which 2 were waited for; matrix products, arithmetic and copies ran while one was open for 2% of the time, Pallas kernels for 0%

commit v1 on v0

--- a/solution.py
+++ b/solution.py
@@ -5,6 +5,19 @@
 
 residual_scale = 2.0**0.25
 norm_eps = 1e-05
+
+
+def collect(shard, axis, dim):
+    size, index, rows = (lax.axis_size(axis), lax.axis_index(axis), shard.shape[dim])
+    upward = [(i, (i + 1) % size) for i in range(size)]
+    whole = jnp.zeros((*shard.shape[:dim], size * rows, *shard.shape[dim + 1 :]), shard.dtype)
+    held = shard
+    for step in range(size):
+        source = (index - step) % size
+        whole = lax.dynamic_update_slice_in_dim(whole, held, source * rows, axis=dim)
+        if step < size - 1:
+            held = lax.ppermute(held, axis, upward)
+    return whole
 
 
 def copy_for_each(array, axis):
@@ -47,7 +60,7 @@
     regrouped = lax.all_to_all(up_weight, "ra", split_axis=1, concat_axis=0, tiled=True)
     pre_share = lax.dot_general(
         regrouped,
-        lax.all_gather(normed, "ra", axis=1, tiled=True),
+        collect(normed, "ra", 1),
         (((0,), (1,)), ((), ())),
         preferred_element_type=jnp.float32,
     )

time: 325 us -> 516 us (1.59)
  waiting for transfers between devices: 163 us -> 364 us
  blocking collectives: 114 us -> 53.4 us
  local copies, waits for them, and re-layouts: 9.57 us -> 47.8 us
  starting transfers between devices: 0.08 us -> 15.4 us
    ppermute x0 -> x15, waiting for transfers between devices: none -> 260 us  [collect(): held = lax.ppermute(held, axis, upward)]
    all_gather x1 -> x0, waiting for transfers between devices: 65.2 us -> none  [per_device(): lax.all_gather(normed, 'ra', axis=1, tiled=True)]
    all_to_all x1 -> x0, blocking collectives: 44.3 us -> none  [per_device(): lax.all_to_all(up_weight, 'ra', split_axis=1, concat_axis=0, tiled=True)]
    dynamic_update_slice x0 -> x15, local copies, waits for them, and re-layouts: none -> 24.2 us  [collect(): lax.dynamic_update_slice_in_dim(whole, held, source * rows, axis=dim)]
    all_to_all x3 -> x2, blocking collectives: 69.5 us -> 53.4 us  [copy_for_each(): lax.all_to_all(jnp.broadcast_to(array[None], (length, *array.shape)), axi...]
    all_to_all x0 -> x2, starting transfers between devices: none -> 14.8 us  [the longest x1 7.99 us: copy_for_each(): lax.all_to_all(jnp.broadcast_to(array[None], (length, *array.shape)), axi...]
    all_to_all x0 -> x2, waiting for transfers between devices: none -> 8.33 us  [the longest x1 8.32 us: copy_for_each(): lax.all_to_all(jnp.broadcast_to(array[None], (length, *array.shape)), axi...]
    unnamed x17 -> x43, local copies, waits for them, and re-layouts: 5.25 us -> 12.4 us
  transfers between devices with their start and end apart: 2 -> 18, of which waited for: 2 -> 17; matrix products, arithmetic and copies ran while one was open for 2% -> 6% of each run, Pallas kernels for 0% -> 0%
where the time goes in v1:
time: 516 us; the launch traced here: 515 us
  waiting for transfers between devices  364 us (71%)
  blocking collectives  53.4 us (10%)
  local copies, waits for them, and re-layouts  47.8 us (9%)
  starting transfers between devices  15.4 us (3%)
  matrix products  13.9 us (3%)
  between operations  13.6 us (3%)
  other arithmetic  7.56 us (1%)
    ppermute x15, waiting for transfers between devices, collect(): held = lax.ppermute(held, axis, upward)  260 us
    all_gather x1, waiting for transfers between devices, per_device(): lax.all_gather(hidden_share, 'ra', axis=0, tiled=True)  95.2 us
    all_to_all x2, blocking collectives, copy_for_each(): lax.all_to_all(jnp.broadcast_to(array[None], (length, *array.shape)), axi...  53.4 us
    dynamic_update_slice x15, local copies, waits for them, and re-layouts, collect(): lax.dynamic_update_slice_in_dim(whole, held, source * rows, axis=dim)  24.2 us
    unnamed x43, local copies, waits for them, and re-layouts  12.4 us
  transfers between devices with their start and end apart: 18, of which 17 were waited for; matrix products, arithmetic and copies ran while one was open for 6% of the time, Pallas kernels for 0%

profile of v1, /device:TPU:0, one launch (start us, length us, event | category | flops | bytes accessed | tf_op | source)
XLA Modules:
  0.0 515.3 jit_solution(12768475944955270042)
XLA Ops:
  6.5 2.1 fusion.3
  9.4 8.0 %all-to-all-start = ((f32[16,1,3072]{2,1,0:T(1,128)}), f32[16,1,3072]{2,1,0:T(1,128)S(1)}, u32[]{:S(2)}, u32[]{:S(2)}) async-start(f32[16,1,3072]{2,1,0:T(1,128)} %broadcast_in_dim.8), calls=%async_computation | async-start | bytes 393216 | tf_op jit(solution)/shard_map/all_to_all | solution.py:25
  17.4 8.3 %all-to-all-done = f32[16,1,3072]{2,1,0:T(1,128)S(1)} async-done(((f32[16,1,3072]{2,1,0:T(1,128)}), f32[16,1,3072]{2,1,0:T(1,128)S(1)}, u32[]{:S(2)}, u32[]{:S(2)}) %all-to-all-start) | async-done | bytes 196640 | tf_op jit(solution)/shard_map/all_to_all | solution.py:25
  25.9 6.1 %broadcast_in_dim.9 = bf16[1536,4096]{1,0:T(8,128)(2,1)} broadcast(bf16[]{:T(256)} %constant.121.clone.1), dimensions={} | broadcast | bytes 12582914 | tf_op jit(solution)/shard_map/broadcast_in_dim | solution.py:13
  32.1 1.5 constant_dynamic-update-slice_fusion.15
  34.1 20.6 %collective-permute-done = bf16[1536,256]{1,0:T(8,128)(2,1)S(1)} collective-permute-done((bf16[1536,256]{1,0:T(8,128)(2,1)S(1)}, bf16[1536,256]{1,0:T(8,128)(2,1)S(1)}, u32[]{:S(2)}, u32[]{:S(2)}) %collective-permute-start) | collective-permute-done | bytes 786464 | tf_op jit(solution)/shard_map/ppermute | solution.py:19
  55.6 19.4 %collective-permute-done.1 = bf16[1536,256]{1,0:T(8,128)(2,1)S(1)} collective-permute-done((bf16[1536,256]{1,0:T(8,128)(2,1)S(1)}, bf16[1536,256]{1,0:T(8,128)(2,1)S(1)}, u32[]{:S(2)}, u32[]{:S(2)}) %collective-permute-start.1) | collective-permute-done | bytes 786464 | tf_op jit(solution)/shard_map/ppermute | solution.py:19
  75.0 0.9 copy-done.16
  75.9 18.5 %collective-permute-done.2 = bf16[1536,256]{1,0:T(8,128)(2,1)S(1)} collective-permute-done((bf16[1536,256]{1,0:T(8,128)(2,1)S(1)}, bf16[1536,256]{1,0:T(8,128)(2,1)S(1)}, u32[]{:S(2)}, u32[]{:S(2)}) %collective-permute-start.2) | collective-permute-done | bytes 786464 | tf_op jit(solution)/shard_map/ppermute | solution.py:19
  95.3 18.6 %collective-permute-done.3 = bf16[1536,256]{1,0:T(8,128)(2,1)S(1)} collective-permute-done((bf16[1536,256]{1,0:T(8,128)(2,1)S(1)}, bf16[1536,256]{1,0:T(8,128)(2,1)S(1)}, u32[]{:S(2)}, u32[]{:S(2)}) %collective-permute-start.3) | collective-permute-done | bytes 786464 | tf_op jit(solution)/shard_map/ppermute | solution.py:19
  114.8 17.7 %collective-permute-done.4 = bf16[1536,256]{1,0:T(8,128)(2,1)S(1)} collective-permute-done((bf16[1536,256]{1,0:T(8,128)(2,1)S(1)}, bf16[1536,256]{1,0:T(8,128)(2,1)S(1)}, u32[]{:S(2)}, u32[]{:S(2)}) %collective-permute-start.4) | collective-permute-done | bytes 786464 | tf_op jit(solution)/shard_map/ppermute | solution.py:19
  133.5 16.8 %collective-permute-done.5 = bf16[1536,256]{1,0:T(8,128)(2,1)S(1)} collective-permute-done((bf16[1536,256]{1,0:T(8,128)(2,1)S(1)}, bf16[1536,256]{1,0:T(8,128)(2,1)S(1)}, u32[]{:S(2)}, u32[]{:S(2)}) %collective-permute-start.5) | collective-permute-done | bytes 786464 | tf_op jit(solution)/shard_map/ppermute | solution.py:19
  150.3 0.9 copy-done.14
  151.2 15.9 %collective-permute-done.6 = bf16[1536,256]{1,0:T(8,128)(2,1)S(1)} collective-permute-done((bf16[1536,256]{1,0:T(8,128)(2,1)S(1)}, bf16[1536,256]{1,0:T(8,128)(2,1)S(1)}, u32[]{:S(2)}, u32[]{:S(2)}) %collective-permute-start.6) | collective-permute-done | bytes 786464 | tf_op jit(solution)/shard_map/ppermute | solution.py:19
  168.0 17.2 %collective-permute-done.7 = bf16[1536,256]{1,0:T(8,128)(2,1)S(1)} collective-permute-done((bf16[1536,256]{1,0:T(8,128)(2,1)S(1)}, bf16[1536,256]{1,0:T(8,128)(2,1)S(1)}, u32[]{:S(2)}, u32[]{:S(2)}) %collective-permute-start.7) | collective-permute-done | bytes 786464 | tf_op jit(solution)/shard_map/ppermute | solution.py:19
  185.2 0.9 copy-done.12
  186.1 19.1 %collective-permute-done.8 = bf16[1536,256]{1,0:T(8,128)(2,1)} collective-permute-done((bf16[1536,256]{1,0:T(8,128)(2,1)S(1)}, bf16[1536,256]{1,0:T(8,128)(2,1)}, u32[]{:S(2)}, u32[]{:S(2)}) %collective-permute-start.8) | collective-permute-done | bytes 786464 | tf_op jit(solution)/shard_map/ppermute | solution.py:19
  205.2 4.1 copy.14
  209.3 6.8 %all-to-all-start.1 = ((bf16[256,16,256]{0,2,1:T(8,128)(2,1)}), bf16[256,16,256]{0,2,1:T(8,128)(2,1)}, u32[]{:S(2)}, u32[]{:S(2)}) async-start(bf16[256,16,256]{0,2,1:T(8,128)(2,1)} %bitcast.9), calls=%async_computation.1 | async-start | bytes 4194304 | tf_op jit(solution)/shard_map/all_to_all | solution.py:60
  216.1 22.2 %collective-permute-done.9 = bf16[1536,256]{1,0:T(8,128)(2,1)} collective-permute-done((bf16[1536,256]{1,0:T(8,128)(2,1)}, bf16[1536,256]{1,0:T(8,128)(2,1)}, u32[]{:S(2)}, u32[]{:S(2)}) %collective-permute-start.9) | collective-permute-done | bytes 786464 | tf_op jit(solution)/shard_map/ppermute | solution.py:19
  238.3 23.7 %collective-permute-done.10 = bf16[1536,256]{1,0:T(8,128)(2,1)} collective-permute-done((bf16[1536,256]{1,0:T(8,128)(2,1)}, bf16[1536,256]{1,0:T(8,128)(2,1)}, u32[]{:S(2)}, u32[]{:S(2)}) %collective-permute-start.10) | collective-permute-done | bytes 786464 | tf_op jit(solution)/shard_map/ppermute | solution.py:19
  261.9 2.1 constant_dynamic-update-slice_fusion.14
  264.1 2.1 constant_dynamic-update-slice_fusion.13
  266.2 3.9 copy.15
  270.1 11.3 %collective-permute-done.11 = bf16[1536,256]{1,0:T(8,128)(2,1)} collective-permute-done((bf16[1536,256]{1,0:T(8,128)(2,1)}, bf16[1536,256]{1,0:T(8,128)(2,1)}, u32[]{:S(2)}, u32[]{:S(2)}) %collective-permute-start.11) | collective-permute-done | bytes 786464 | tf_op jit(solution)/shard_map/ppermute | solution.py:19
  281.5 2.1 constant_dynamic-update-slice_fusion.12
  283.6 2.2 constant_dynamic-update-slice_fusion.11
  285.8 1.0 constant_dynamic-update-slice_fusion.10
  286.8 1.0 constant_dynamic-update-slice_fusion.9
  287.8 14.6 %collective-permute-done.12 = bf16[1536,256]{1,0:T(8,128)(2,1)S(1)} collective-permute-done((bf16[1536,256]{1,0:T(8,128)(2,1)}, bf16[1536,256]{1,0:T(8,128)(2,1)S(1)}, u32[]{:S(2)}, u32[]{:S(2)}) %collective-permute-start.12) | collective-permute-done | bytes 786464 | tf_op jit(solution)/shard_map/ppermute | solution.py:19
  302.4 1.0 constant_dynamic-update-slice_fusion.8
  303.4 1.0 constant_dynamic-update-slice_fusion.7
  304.4 2.1 constant_dynamic-update-slice_fusion.6
  306.5 2.1 constant_dynamic-update-slice_fusion.5
  308.6 15.6 %collective-permute-done.13 = bf16[1536,256]{1,0:T(8,128)(2,1)S(1)} collective-permute-done((bf16[1536,256]{1,0:T(8,128)(2,1)S(1)}, bf16[1536,256]{1,0:T(8,128)(2,1)S(1)}, u32[]{:S(2)}, u32[]{:S(2)}) %collective-permute-start.13) | collective-permute-done | bytes 786464 | tf_op jit(solution)/shard_map/ppermute | solution.py:19
  324.2 2.1 constant_dynamic-update-slice_fusion.4
  326.3 2.3 constant_dynamic-update-slice_fusion.3
  328.6 1.0 constant_dynamic-update-slice_fusion.2
  329.6 1.0 constant_dynamic-update-slice_fusion.1
  330.6 8.9 %collective-permute-done.14 = bf16[1536,256]{1,0:T(8,128)(2,1)S(1)} collective-permute-done((bf16[1536,256]{1,0:T(8,128)(2,1)S(1)}, bf16[1536,256]{1,0:T(8,128)(2,1)S(1)}, u32[]{:S(2)}, u32[]{:S(2)}) %collective-permute-start.14) | collective-permute-done | bytes 786464 | tf_op jit(solution)/shard_map/ppermute | solution.py:19
  339.5 1.0 constant_dynamic-update-slice_fusion
  340.5 7.4 %fusion.2 = bf16[256,1536]{0,1:T(8,128)(2,1)} fusion(bf16[1536,4096]{1,0:T(8,128)(2,1)} %constant_dynamic-update-slice_fusion, bf16[4096,256]{1,0:T(8,128)(2,1)S(1)} %bitcast.10), kind=kOutput, calls=%fused_computation.5 | convolution fusion | flops 3222405120 | bytes 15466496 | tf_op jit(solution)/shard_map/dot_general | solution.py:61
  348.0 95.2 %all-gather.2.cloned.1.call-done = bf16[4096,1536]{0,1:T(8,128)(2,1)} async-done(((bf16[256,1536]{0,1:T(8,128)(2,1)}), bf16[4096,1536]{0,1:T(8,128)(2,1)}) %all-gather.2.cloned.1.call-update) | async-done | bytes 12582928 | tf_op jit(solution)/shard_map/all_gather | solution.py:69
  443.2 6.5 %convolution_convert_fusion = bf16[1536,256]{1,0:T(8,128)(2,1)S(1)} fusion(bf16[4096,1536]{0,1:T(8,128)(2,1)} %all-gather.2.cloned.1.call-done, bf16[4096,256]{1,0:T(8,128)(2,1)S(1)} %copy-done), kind=kOutput, calls=%fused_computation.4 | convolution fusion | flops 3221618688 | bytes 15466496 | tf_op jit(solution)/shard_map/dot_general | solution.py:68
  449.9 40.3 %all_to_all.36 = bf16[4,1536,256]{2,1,0:T(8,128)(2,1)S(1)} all-to-all(bf16[4,1536,256]{2,1,0:T(8,128)(2,1)S(1)} %broadcast_in_dim.10), channel_id=1, replica_groups=mesh['ra'=16,'cb'=4,'dp'=2] {'cb'}, dimensions={0} | all-to-all | bytes 6291456 | tf_op jit(solution)/shard_map/all_to_all | solution.py:25
  490.6 1.2 copy-done.1
  492.5 13.1 %all_to_all.37 = f32[16,1,3072]{2,1,0:T(1,128)S(1)} all-to-all(f32[16,1,3072]{2,1,0:T(1,128)S(1)} %broadcast_in_dim.11), channel_id=1, replica_groups=mesh['ra'=16,'cb'=4,'dp'=2] {'ra'}, dimensions={0} | all-to-all | bytes 393216 | tf_op jit(solution)/shard_map/all_to_all | solution.py:25
  505.7 2.8 add_convert_fusion
  (67 shorter events, 7.5 us)
Async XLA Ops:
  6.5 436.6 %copy-start = (bf16[4096,256]{1,0:T(8,128)(2,1)S(1)}, bf16[4096,256]{1,0:T(8,128)(2,1)}, u32[]{:S(2)}) copy-start(bf16[4096,256]{1,0:T(8,128)(2,1)} %param.13) | copy-start | bytes 6291460
  9.4 16.3 %all-to-all-start = ((f32[16,1,3072]{2,1,0:T(1,128)}), f32[16,1,3072]{2,1,0:T(1,128)S(1)}, u32[]{:S(2)}, u32[]{:S(2)}) async-start(f32[16,1,3072]{2,1,0:T(1,128)} %broadcast_in_dim.8), calls=%async_computation | async-start | bytes 393216 | tf_op jit(solution)/shard_map/all_to_all | solution.py:25
  25.9 6.2 %copy-start.2 = (bf16[1536,256]{1,0:T(8,128)(2,1)S(1)}, bf16[1536,256]{1,0:T(8,128)(2,1)}, u32[]{:S(2)}) copy-start(bf16[1536,256]{1,0:T(8,128)(2,1)} %param.9) | copy-start | bytes 2359300
  25.9 6.2 %copy-start.3 = (bf16[1536,256]{1,0:T(8,128)(2,1)S(1)}, bf16[1536,256]{1,0:T(8,128)(2,1)}, u32[]{:S(2)}) copy-start(bf16[1536,256]{1,0:T(8,128)(2,1)} %param.8) | copy-start | bytes 2359300
  25.9 6.1 %copy-start.17 = (f32[256]{0:T(256)S(1)}, f32[256]{0:T(256)}, u32[]{:S(2)}) copy-start(f32[256]{0:T(256)} %param.11) | copy-start | bytes 3076
  25.9 6.1 %copy-start.18 = (f32[256]{0:T(256)S(1)}, f32[256]{0:T(256)}, u32[]{:S(2)}) copy-start(f32[256]{0:T(256)} %param.10) | copy-start | bytes 3076
  33.5 21.2 %collective-permute-start = (bf16[1536,256]{1,0:T(8,128)(2,1)S(1)}, bf16[1536,256]{1,0:T(8,128)(2,1)S(1)}, u32[]{:S(2)}, u32[]{:S(2)}) collective-permute-start(bf16[1536,256]{1,0:T(8,128)(2,1)S(1)} %get-tuple-element.10), channel_id=1, source_target_pairs={{0,8},{8,16},{16,24},{24,32},{32,40},{40,48},{48,56},{56,64},{64,7... | collective-permute-start | bytes 2359304 | tf_op jit(solution)/shard_map/ppermute | solution.py:19
  54.7 0.9 copy-start.11
  54.7 20.3 %collective-permute-start.1 = (bf16[1536,256]{1,0:T(8,128)(2,1)S(1)}, bf16[1536,256]{1,0:T(8,128)(2,1)S(1)}, u32[]{:S(2)}, u32[]{:S(2)}) collective-permute-start(bf16[1536,256]{1,0:T(8,128)(2,1)S(1)} %collective-permute-done), channel_id=1, source_target_pairs={{0,8},{8,16},{16,24},{24,32},{32,40},{40,48},{48,56},{56,64},{64,7... | collective-permute-start | bytes 2359304 | tf_op jit(solution)/shard_map/ppermute | solution.py:19
  75.0 0.9 copy-start.16
  75.0 19.5 %collective-permute-start.2 = (bf16[1536,256]{1,0:T(8,128)(2,1)S(1)}, bf16[1536,256]{1,0:T(8,128)(2,1)S(1)}, u32[]{:S(2)}, u32[]{:S(2)}) collective-permute-start(bf16[1536,256]{1,0:T(8,128)(2,1)S(1)} %collective-permute-done.1), channel_id=1, source_target_pairs={{0,8},{8,16},{16,24},{24,32},{32,40},{40,48},{48,56},{56,64},{64,7... | collective-permute-start | bytes 2359304 | tf_op jit(solution)/shard_map/ppermute | solution.py:19
  94.5 0.9 copy-start.5
  95.3 18.6 %collective-permute-start.3 = (bf16[1536,256]{1,0:T(8,128)(2,1)S(1)}, bf16[1536,256]{1,0:T(8,128)(2,1)S(1)}, u32[]{:S(2)}, u32[]{:S(2)}) collective-permute-start(bf16[1536,256]{1,0:T(8,128)(2,1)S(1)} %collective-permute-done.2), channel_id=1, source_target_pairs={{0,8},{8,16},{16,24},{24,32},{32,40},{40,48},{48,56},{56,64},{64,7... | collective-permute-start | bytes 2359304 | tf_op jit(solution)/shard_map/ppermute | solution.py:19
  113.9 0.9 copy-start.6
  114.8 17.7 %collective-permute-start.4 = (bf16[1536,256]{1,0:T(8,128)(2,1)S(1)}, bf16[1536,256]{1,0:T(8,128)(2,1)S(1)}, u32[]{:S(2)}, u32[]{:S(2)}) collective-permute-start(bf16[1536,256]{1,0:T(8,128)(2,1)S(1)} %collective-permute-done.3), channel_id=1, source_target_pairs={{0,8},{8,16},{16,24},{24,32},{32,40},{40,48},{48,56},{56,64},{64,7... | collective-permute-start | bytes 2359304 | tf_op jit(solution)/shard_map/ppermute | solution.py:19
  132.6 0.9 copy-start.9
  132.6 17.7 %collective-permute-start.5 = (bf16[1536,256]{1,0:T(8,128)(2,1)S(1)}, bf16[1536,256]{1,0:T(8,128)(2,1)S(1)}, u32[]{:S(2)}, u32[]{:S(2)}) collective-permute-start(bf16[1536,256]{1,0:T(8,128)(2,1)S(1)} %collective-permute-done.4), channel_id=1, source_target_pairs={{0,8},{8,16},{16,24},{24,32},{32,40},{40,48},{48,56},{56,64},{64,7... | collective-permute-start | bytes 2359304 | tf_op jit(solution)/shard_map/ppermute | solution.py:19
  150.3 0.9 copy-start.14
  150.3 16.8 %collective-permute-start.6 = (bf16[1536,256]{1,0:T(8,128)(2,1)S(1)}, bf16[1536,256]{1,0:T(8,128)(2,1)S(1)}, u32[]{:S(2)}, u32[]{:S(2)}) collective-permute-start(bf16[1536,256]{1,0:T(8,128)(2,1)S(1)} %collective-permute-done.5), channel_id=1, source_target_pairs={{0,8},{8,16},{16,24},{24,32},{32,40},{40,48},{48,56},{56,64},{64,7... | collective-permute-start | bytes 2359304 | tf_op jit(solution)/shard_map/ppermute | solution.py:19
  167.1 0.9 copy-start.7
  168.0 17.2 %collective-permute-start.7 = (bf16[1536,256]{1,0:T(8,128)(2,1)S(1)}, bf16[1536,256]{1,0:T(8,128)(2,1)S(1)}, u32[]{:S(2)}, u32[]{:S(2)}) collective-permute-start(bf16[1536,256]{1,0:T(8,128)(2,1)S(1)} %collective-permute-done.6), channel_id=1, source_target_pairs={{0,8},{8,16},{16,24},{24,32},{32,40},{40,48},{48,56},{56,64},{64,7... | collective-permute-start | bytes 2359304 | tf_op jit(solution)/shard_map/ppermute | solution.py:19
  185.2 0.9 copy-start.12
  186.1 19.1 %collective-permute-start.8 = (bf16[1536,256]{1,0:T(8,128)(2,1)S(1)}, bf16[1536,256]{1,0:T(8,128)(2,1)}, u32[]{:S(2)}, u32[]{:S(2)}) collective-permute-start(bf16[1536,256]{1,0:T(8,128)(2,1)S(1)} %collective-permute-done.7), channel_id=1, source_target_pairs={{0,8},{8,16},{16,24},{24,32},{32,40},{40,48},{48,56},{56,64},{64,7... | collective-permute-start | bytes 2359304 | tf_op jit(solution)/shard_map/ppermute | solution.py:19
  205.2 33.1 %collective-permute-start.9 = (bf16[1536,256]{1,0:T(8,128)(2,1)}, bf16[1536,256]{1,0:T(8,128)(2,1)}, u32[]{:S(2)}, u32[]{:S(2)}) collective-permute-start(bf16[1536,256]{1,0:T(8,128)(2,1)} %collective-permute-done.8), channel_id=1, source_target_pairs={{0,8},{8,16},{16,24},{24,32},{32,40},{40,48},{48,56},{56,64},{64,7... | collective-permute-start | bytes 2359304 | tf_op jit(solution)/shard_map/ppermute | solution.py:19
  209.3 56.9 %all-to-all-start.1 = ((bf16[256,16,256]{0,2,1:T(8,128)(2,1)}), bf16[256,16,256]{0,2,1:T(8,128)(2,1)}, u32[]{:S(2)}, u32[]{:S(2)}) async-start(bf16[256,16,256]{0,2,1:T(8,128)(2,1)} %bitcast.9), calls=%async_computation.1 | async-start | bytes 4194304 | tf_op jit(solution)/shard_map/all_to_all | solution.py:60
  216.0 227.1 %all-gather.2.cloned.1.call-start = ((), (), s32[]{:S(2)}) async-start(), calls=%async_computation.4 | async-start | bytes 13369344 | tf_op jit(solution)/shard_map/all_gather | solution.py:69
  238.3 23.7 %collective-permute-start.10 = (bf16[1536,256]{1,0:T(8,128)(2,1)}, bf16[1536,256]{1,0:T(8,128)(2,1)}, u32[]{:S(2)}, u32[]{:S(2)}) collective-permute-start(bf16[1536,256]{1,0:T(8,128)(2,1)} %collective-permute-done.9), channel_id=1, source_target_pairs={{0,8},{8,16},{16,24},{24,32},{32,40},{40,48},{48,56},{56,64},{64,7... | collective-permute-start | bytes 2359304 | tf_op jit(solution)/shard_map/ppermute | solution.py:19
  261.9 19.5 %collective-permute-start.11 = (bf16[1536,256]{1,0:T(8,128)(2,1)}, bf16[1536,256]{1,0:T(8,128)(2,1)}, u32[]{:S(2)}, u32[]{:S(2)}) collective-permute-start(bf16[1536,256]{1,0:T(8,128)(2,1)} %collective-permute-done.10), channel_id=1, source_target_pairs={{0,8},{8,16},{16,24},{24,32},{32,40},{40,48},{48,56},{56,64},{64,7... | collective-permute-start | bytes 2359304 | tf_op jit(solution)/shard_map/ppermute | solution.py:19
  270.1 15.7 %copy-start.10 = (bf16[1536,256]{1,0:T(8,128)(2,1)S(1)}, bf16[1536,256]{1,0:T(8,128)(2,1)}, u32[]{:S(2)}) copy-start(bf16[1536,256]{1,0:T(8,128)(2,1)} %copy-done.9) | copy-start | bytes 2359300
  270.1 16.6 %copy-start.15 = (bf16[1536,256]{1,0:T(8,128)(2,1)S(1)}, bf16[1536,256]{1,0:T(8,128)(2,1)}, u32[]{:S(2)}) copy-start(bf16[1536,256]{1,0:T(8,128)(2,1)} %copy-done.14) | copy-start | bytes 2359300
  270.1 32.2 %copy-start.8 = (bf16[1536,256]{1,0:T(8,128)(2,1)S(1)}, bf16[1536,256]{1,0:T(8,128)(2,1)}, u32[]{:S(2)}) copy-start(bf16[1536,256]{1,0:T(8,128)(2,1)} %copy-done.7) | copy-start | bytes 2359300
  281.5 20.9 %collective-permute-start.12 = (bf16[1536,256]{1,0:T(8,128)(2,1)}, bf16[1536,256]{1,0:T(8,128)(2,1)S(1)}, u32[]{:S(2)}, u32[]{:S(2)}) collective-permute-start(bf16[1536,256]{1,0:T(8,128)(2,1)} %collective-permute-done.11), channel_id=1, source_target_pairs={{0,8},{8,16},{16,24},{24,32},{32,40},{40,48},{48,56},{56,64},{64,7... | collective-permute-start | bytes 2359304 | tf_op jit(solution)/shard_map/ppermute | solution.py:19
  283.6 19.8 %copy-start.13 = (bf16[1536,256]{1,0:T(8,128)(2,1)S(1)}, bf16[1536,256]{1,0:T(8,128)(2,1)}, u32[]{:S(2)}) copy-start(bf16[1536,256]{1,0:T(8,128)(2,1)} %copy-done.12) | copy-start | bytes 2359300
  302.4 21.8 %collective-permute-start.13 = (bf16[1536,256]{1,0:T(8,128)(2,1)S(1)}, bf16[1536,256]{1,0:T(8,128)(2,1)S(1)}, u32[]{:S(2)}, u32[]{:S(2)}) collective-permute-start(bf16[1536,256]{1,0:T(8,128)(2,1)S(1)} %collective-permute-done.12), channel_id=1, source_target_pairs={{0,8},{8,16},{16,24},{24,32},{32,40},{40,48},{48,56},{56,64},{64,7... | collective-permute-start | bytes 2359304 | tf_op jit(solution)/shard_map/ppermute | solution.py:19
  324.2 15.3 %collective-permute-start.14 = (bf16[1536,256]{1,0:T(8,128)(2,1)S(1)}, bf16[1536,256]{1,0:T(8,128)(2,1)S(1)}, u32[]{:S(2)}, u32[]{:S(2)}) collective-permute-start(bf16[1536,256]{1,0:T(8,128)(2,1)S(1)} %collective-permute-done.13), channel_id=1, source_target_pairs={{0,8},{8,16},{16,24},{24,32},{32,40},{40,48},{48,56},{56,64},{64,7... | collective-permute-start | bytes 2359304 | tf_op jit(solution)/shard_map/ppermute | solution.py:19
  326.3 14.2 %copy-start.4 = (bf16[16,256,256]{2,1,0:T(8,128)(2,1)S(1)}, bf16[16,256,256]{2,1,0:T(8,128)(2,1)}, u32[]{:S(2)}) copy-start(bf16[16,256,256]{2,1,0:T(8,128)(2,1)} %copy.15) | copy-start | bytes 6291460
  490.2 15.5 %copy-start.19 = (f32[256]{0:T(256)S(1)}, f32[256]{0:T(256)}, u32[]{:S(2)}) copy-start(f32[256]{0:T(256)} %param.15) | copy-start | bytes 3076
  490.2 15.5 %copy-start.20 = (f32[256]{0:T(256)S(1)}, f32[256]{0:T(256)}, u32[]{:S(2)}) copy-start(f32[256]{0:T(256)} %param.14) | copy-start | bytes 3076
  490.6 1.2 copy-start.1
Sparse Core Ops, SparseCore 0:
  348.1 95.0 all-gather.1
